TPU v7x, 32 devices: a whole 2x2x4 slice. The times are simulated.
32 devices in a mesh: sp: 8 (over z, y), tp: 4 (over x, core).
Axes of the slice: x: 2, y: 2, z: 4, core: 2. Of those that a mesh axis runs over, the one named last changes fastest.
Arguments:
- residual: bfloat16 [3072, 2048], P('sp'), may hold values from -50 to 50
- queries_a: bfloat16 [3072, 512], P('sp', 'tp'), may hold values from -50 to 50
- keys_a: bfloat16 [3072, 512], P('sp', 'tp'), may hold values from -9 to 9
- values_a: bfloat16 [3072, 512], P('sp', 'tp'), may hold values from -6 to 6
- queries_b: bfloat16 [3072, 1024], P('sp', 'tp'), may hold values from -50 to 50
- keys_b: bfloat16 [3072, 1024], P('sp', 'tp'), may hold values from -9 to 9
- values_b: bfloat16 [3072, 512], P('sp', 'tp'), may hold values from -6 to 6
- mix_lambda: float32 [2, 4], P(None, 'tp'), may hold values from 0.3 to 0.8
- head_gain: float32 [2, 128], replicated, may hold values from 0.1 to 1.9
- out_a: bfloat16 [512, 2048], P('tp'), may hold values from -0.1875 to 0.1875
- out_b: bfloat16 [512, 2048], P('tp'), may hold values from -0.1875 to 0.1875
- norm_gain: float32 [2048], replicated, may hold values from 0.1 to 1.9
- w_gate: bfloat16 [2048, 5632], P('sp', 'tp'), may hold values from -0.125 to 0.125
- w_up: bfloat16 [2048, 5632], P('sp', 'tp'), may hold values from -0.125 to 0.125
- w_down: bfloat16 [5632, 2048], P('tp', 'sp'), may hold values from -0.21875 to 0.21875
Outputs:
- layer_out: bfloat16 [3072, 2048], P('sp', 'tp')
All inputs are finite; a program needn't handle non-finite values.
Results may differ from a plain program's by a relative error of at most 0.0085.
Values may be sent and summed in bfloat16 or wider, within the bound.
A program may use at most 256 MiB of HBM per device.

v0:
```python
import jax
import jax.numpy as jnp
from jax import lax
from jax.sharding import PartitionSpec as P

eps_norm = 1e-06
head_scale = 0.8


def group_update(carry, queries, keys, values):
    peak, denom, numer = carry
    rows = queries.shape[0]
    heads = peak.shape[1]
    width = queries.shape[1] // (2 * heads)
    count = keys.shape[0]
    query_rows = queries.reshape(rows, heads, 2, width)
    key_rows = keys.reshape(count, heads, 2, width)
    value_rows = values.reshape(count, heads, values.shape[1] // heads)
    peaks, denoms, numers = ([], [], [])
    for which in range(2):
        scores = jnp.einsum(
            "qhe,khe->hqk",
            query_rows[:, :, which],
            key_rows[:, :, which],
            preferred_element_type=jnp.float32,
        ) * width ** (-0.5)
        fresh = jnp.max(scores, axis=-1)
        decay = jnp.exp(peak[which] - fresh)
        weights = jnp.exp(scores - fresh[..., None])
        denoms.append(denom[which] * decay + jnp.sum(weights, axis=-1))
        added = jnp.einsum(
            "hqk,khv->hqv",
            weights.astype(jnp.bfloat16),
            value_rows,
            preferred_element_type=jnp.float32,
        )
        numers.append(numer[which] * decay[..., None] + added)
        peaks.append(fresh)
    return (jnp.stack(peaks), jnp.stack(denoms), jnp.stack(numers))


def finish(carry, lambdas, gain):
    peak, denom, numer = carry
    ratio = numer / denom[..., None]
    mixed = ratio[0] - lambdas[:, None, None] * ratio[1]
    inverse = lax.rsqrt(jnp.mean(mixed * mixed, axis=-1, keepdims=True) + eps_norm)
    normed = mixed * inverse * gain * head_scale
    return jnp.transpose(normed, (1, 0, 2)).reshape(normed.shape[1], -1).astype(jnp.bfloat16)


def local(
    residual,
    queries_a,
    keys_a,
    values_a,
    queries_b,
    keys_b,
    values_b,
    mix_lambda,
    head_gain,
    out_a,
    out_b,
    norm_gain,
    w_gate,
    w_up,
    w_down,
):
    tokens = residual.shape[0]
    width_all = residual.shape[1]
    heads = mix_lambda.shape[1]
    full_out_a, full_out_b = (
        lax.all_gather(out_a, "tp", axis=0, tiled=True),
        lax.all_gather(out_b, "tp", axis=0, tiled=True),
    )

    def start_carry(values):
        return (
            jnp.full((2, heads, tokens), -jnp.inf, jnp.float32),
            jnp.zeros((2, heads, tokens), jnp.float32),
            jnp.zeros((2, heads, tokens, values.shape[1] // heads), jnp.float32),
        )

    carry = start_carry(values_a) + start_carry(values_b)
    pieces = (
        lax.all_gather(keys_a, "sp", axis=0, tiled=True),
        lax.all_gather(keys_b, "sp", axis=0, tiled=True),
        lax.all_gather(values_a, "sp", axis=0, tiled=True),
        lax.all_gather(values_b, "sp", axis=0, tiled=True),
    )
    first = group_update(carry[:3], queries_a, pieces[0], pieces[2])
    second = group_update(carry[3:], queries_b, pieces[1], pieces[3])
    carry = first + second
    heads_a = finish(carry[:3], mix_lambda[0], head_gain[0])
    heads_b = finish(carry[3:], mix_lambda[1], head_gain[1])
    share = width_all // lax.axis_size("tp")
    offset = lax.axis_index("tp") * share
    rows_a, rows_b = (
        lax.all_gather(heads_a, "tp", axis=1, tiled=True),
        lax.all_gather(heads_b, "tp", axis=1, tiled=True),
    )
    projected = jnp.dot(rows_a, full_out_a, preferred_element_type=jnp.float32)
    projected = projected + jnp.dot(rows_b, full_out_b, preferred_element_type=jnp.float32)
    summed = residual.astype(jnp.float32) + projected
    inverse = lax.rsqrt(jnp.mean(summed * summed, axis=-1, keepdims=True) + eps_norm)
    normed = (summed * inverse * norm_gain).astype(jnp.bfloat16)
    summed_cols = lax.dynamic_slice_in_dim(summed, offset, share, 1)
    pieces = (
        lax.all_gather(w_gate, "sp", axis=0, tiled=True),
        lax.all_gather(w_up, "sp", axis=0, tiled=True),
    )
    gate = jnp.dot(normed, pieces[0], preferred_element_type=jnp.float32)
    upward = jnp.dot(normed, pieces[1], preferred_element_type=jnp.float32)
    hidden = (jax.nn.silu(gate) * upward).astype(jnp.bfloat16)
    channel = jnp.dot(
        hidden, lax.all_gather(w_down, "sp", axis=1, tiled=True), preferred_element_type=jnp.float32
    )
    mixed_cols = lax.psum_scatter(
        channel.astype(jnp.bfloat16), "tp", scatter_dimension=1, tiled=True
    ).astype(jnp.float32)
    return (summed_cols + 0.5 * mixed_cols).astype(jnp.bfloat16)


def solution(mesh):
    in_specs = (
        P("sp", None),
        P("sp", "tp"),
        P("sp", "tp"),
        P("sp", "tp"),
        P("sp", "tp"),
        P("sp", "tp"),
        P("sp", "tp"),
        P(None, "tp"),
        P(),
        P("tp", None),
        P("tp", None),
        P(),
        P("sp", "tp"),
        P("sp", "tp"),
        P("tp", "sp"),
    )
    out_specs = P("sp", "tp")
    return jax.shard_map(local, mesh=mesh, in_specs=in_specs, out_specs=out_specs, check_vma=False)
```

profile of v0, /device:TPU:0, one launch (start us, length us, event | category | flops | bytes accessed | tf_op | source)
XLA Modules:
  0.0 440.1 jit_solution(14173542479155542728)
XLA Ops:
  6.5 0.0 all-gather.9.cloned.1.call-start
  6.5 1.8 copy.22
  8.3 0.0 all-gather.9.cloned.1.call-update
  8.4 0.0 all-gather.7.cloned.1.call-start
  8.4 0.7 all-gather.7.cloned.1.call-update
  9.1 0.0 all-gather.11.cloned.1.call-start
  9.2 0.7 all-gather.11.cloned.1.call-update
  9.8 0.0 all-gather.13.cloned.1.call-start
  9.9 0.5 all-gather.13.cloned.1.call-update
  10.4 0.0 all-gather.15.cloned.1.call-start
  10.5 0.5 all-gather.15.cloned.1.call-update
  11.0 0.0 all-gather.17.cloned.1.call-start
  11.1 0.5 all-gather.17.cloned.1.call-update
  11.6 0.0 reduce-scatter.2.cloned.1.call-start
  11.6 0.0 copy-done.5
  11.6 0.1 copy.19
  11.8 35.7 %all_gather.33 = bf16[3072,128]{0,1:T(8,128)(2,1)S(1)} all-gather(bf16[384,128]{0,1:T(8,128)(2,1)S(1)} %copy.19), channel_id=1, replica_groups=mesh['sp'=8,'tp'=4] {'sp'}, dimensions={0}, use_global_device_ids=true | all-gather | bytes 884736 | tf_op jit(solution)/shard_map/all_gather | solution.py:85
  47.5 0.0 copy-done.2
  47.5 0.2 copy.20
  47.7 0.0 copy-done.6
  47.7 0.1 copy.18
  47.8 0.9 fusion.61
  48.7 0.8 fusion
  49.5 0.9 fusion.60
  50.4 0.0 copy-start.3
  50.4 0.8 fusion.2
  51.2 0.0 copy-done.7
  51.2 0.6 fusion.59
  51.9 0.0 copy-done.3
  51.9 32.9 %all_gather.34 = bf16[3072,128]{1,0:T(8,128)(2,1)S(1)} all-gather(bf16[384,128]{1,0:T(8,128)(2,1)S(1)} %copy-done.3), channel_id=1, replica_groups=mesh['sp'=8,'tp'=4] {'sp'}, dimensions={0}, use_global_device_ids=true | all-gather | bytes 884736 | tf_op jit(solution)/shard_map/all_gather | solution.py:87
  84.7 1.1 fusion.24
  85.8 0.0 copy-start.8
  85.8 0.0 copy-start.4
  85.8 1.1 fusion.30
  86.9 0.7 multiply_reduce_fusion.2
  87.6 0.0 copy-done.8
  87.6 0.7 fusion.52
  88.3 7.2 %all_gather.35 = bf16[384,512]{0,1:T(8,128)(2,1)} all-gather(bf16[384,128]{0,1:T(8,128)(2,1)S(1)} %fusion.52), channel_id=1, replica_groups=mesh['sp'=8,'tp'=4] {'tp'}, dimensions={1}, use_global_device_ids=true | all-gather | bytes 491520 | tf_op jit(solution)/shard_map/all_gather | solution.py:98
  95.5 0.0 copy-done.4
  95.5 32.0 %all_gather.38 = bf16[3072,128]{1,0:T(8,128)(2,1)S(1)} all-gather(bf16[384,128]{1,0:T(8,128)(2,1)S(1)} %copy-done.4), channel_id=1, replica_groups=mesh['sp'=8,'tp'=4] {'sp'}, dimensions={0}, use_global_device_ids=true | all-gather | bytes 884736 | tf_op jit(solution)/shard_map/all_gather | solution.py:88
  127.5 2.0 fusion.63
  129.5 0.8 fusion.4
  130.3 0.6 copy-done.1
  131.0 0.9 fusion.62
  131.8 0.8 fusion.6
  132.7 1.0 fusion.36
  133.7 1.0 fusion.42
  134.8 0.7 multiply_reduce_fusion.1
  135.5 0.7 fusion.49
  136.2 6.3 %all_gather.39 = bf16[384,512]{0,1:T(8,128)(2,1)S(1)} all-gather(bf16[384,128]{0,1:T(8,128)(2,1)S(1)} %fusion.49), channel_id=1, replica_groups=mesh['sp'=8,'tp'=4] {'tp'}, dimensions={1}, use_global_device_ids=true | all-gather | bytes 491520 | tf_op jit(solution)/shard_map/all_gather | solution.py:99
  142.5 2.7 fusion.64
  145.3 0.0 copy-start.9
  145.3 0.0 all-gather.11.cloned.1.call-done
  145.3 4.9 %multiply_reduce_fusion = (f32[384]{0:T(512)S(1)}, f32[384,2048]{1,0:T(8,128)}) fusion(f32[384,2048]{1,0:T(8,128)S(1)} %fusion.64, bf16[384,512]{0,1:T(8,128)(2,1)S(1)} %all_gather.39, bf16[512,2048]{1,0:T(8,128)(2,1)} %all-gather.11.cloned.1.call-done, bf16[384,2048]{1,0:T(8,128)(2,1)} %param.15), kind=kOutput, calls=%fused_computation.17 | convolution fusion | flops 809238144 | bytes 10356224 | tf_op jit(solution)/shard_map/dot_general | solution.py:102
  150.3 57.6 %all-gather.13.cloned.1.call-done = bf16[2048,1408]{1,0:T(8,128)(2,1)} async-done(((bf16[256,1408]{1,0:T(8,128)(2,1)}), bf16[2048,1408]{1,0:T(8,128)(2,1)}) %all-gather.13.cloned.1.call-update) | async-done | bytes 5767184 | tf_op jit(solution)/shard_map/all_gather | solution.py:108
  207.9 0.0 copy-done.9
  207.9 7.8 %fusion.58 = f32[384,1408]{1,0:T(8,128)} fusion(bf16[2048,1408]{1,0:T(8,128)(2,1)} %all-gather.13.cloned.1.call-done, f32[384,2048]{1,0:T(8,128)} %get-tuple-element.26, f32[2048]{0:T(1024)S(1)} %copy-done.9, f32[384]{0:T(512)S(1)} %add_rsqrt_fusion), kind=kOutput, calls=%fused_computation.79 | convolution fusion | flops 2216951808 | bytes 11085312 | tf_op jit(solution)/shard_map/dot_general | solution.py:111
  215.7 84.8 %all-gather.15.cloned.1.call-done = bf16[2048,1408]{1,0:T(8,128)(2,1)} async-done(((bf16[256,1408]{1,0:T(8,128)(2,1)}), bf16[2048,1408]{1,0:T(8,128)(2,1)}) %all-gather.15.cloned.1.call-update) | async-done | bytes 5767184 | tf_op jit(solution)/shard_map/all_gather | solution.py:109
  300.5 93.2 %all-gather.17.cloned.1.call-done = bf16[1408,2048]{1,0:T(8,128)(2,1)} async-done(((bf16[1408,256]{1,0:T(8,128)(2,1)}), bf16[1408,2048]{1,0:T(8,128)(2,1)}) %all-gather.17.cloned.1.call-update) | async-done | bytes 5767184 | tf_op jit(solution)/shard_map/all_gather | solution.py:115
  393.7 0.0 copy-done
  393.7 11.2 %convolution_convert_fusion = bf16[384,2048]{1,0:T(8,128)(2,1)} fusion(bf16[1408,2048]{1,0:T(8,128)(2,1)} %all-gather.17.cloned.1.call-done, bf16[2048,1408]{1,0:T(8,128)(2,1)} %all-gather.15.cloned.1.call-done, f32[384,1408]{1,0:T(8,128)} %fusion.58, f32[384,2048]{1,0:T(8,128)S(1)} %copy-done, f32[2048]{0:T(1024)S(1)} %copy-done.9, f32[384]{0:T(512)S(1)} %add_rsqrt_fusion), kind=kOutput, calls=%fused_computation.21 | convolution fusion | flops 4435574784 | bytes 18425344 | tf_op jit(solution)/shard_map/dot_general | solution.py:114
  404.9 0.0 reduce-scatter.2.cloned.1.call-update
  405.0 26.4 %reduce-scatter.2.cloned.1.call-done = bf16[384,512]{1,0:T(8,128)(2,1)} async-done(((bf16[384,2048]{1,0:T(8,128)(2,1)}), bf16[384,512]{1,0:T(8,128)(2,1)}) %reduce-scatter.2.cloned.1.call-update) | async-done | bytes 393232 | tf_op jit(solution)/shard_map/reduce_scatter | solution.py:117
  431.4 1.9 add_convert_fusion
  (24 shorter events, 0.2 us)
Async XLA Ops:
  6.5 5.1 %copy-start.5 = (bf16[384,128]{1,0:T(8,128)(2,1)S(1)}, bf16[384,128]{1,0:T(8,128)(2,1)}, u32[]{:S(2)}) copy-start(bf16[384,128]{1,0:T(8,128)(2,1)} %param.17) | copy-start | bytes 294916
  6.5 41.0 %copy-start.2 = (bf16[384,256]{1,0:T(8,128)(2,1)S(1)}, bf16[384,256]{1,0:T(8,128)(2,1)}, u32[]{:S(2)}) copy-start(bf16[384,256]{1,0:T(8,128)(2,1)} %param.19) | copy-start | bytes 589828
  6.5 41.1 %copy-start.6 = (bf16[384,128]{1,0:T(8,128)(2,1)S(1)}, bf16[384,128]{1,0:T(8,128)(2,1)}, u32[]{:S(2)}) copy-start(bf16[384,128]{1,0:T(8,128)(2,1)} %param.16) | copy-start | bytes 294916
  6.5 121.0 %all-gather.9.cloned.1.call-start = ((), (), s32[]{:S(2)}) async-start(), calls=%async_computation.2 | async-start | bytes 1769472 | tf_op jit(solution)/shard_map/all_gather | solution.py:86
  8.4 134.2 %all-gather.7.cloned.1.call-start = ((), (), s32[]{:S(2)}) async-start(), calls=%async_computation.1 | async-start | bytes 2621440 | tf_op jit(solution)/shard_map/all_gather | solution.py:72
  9.1 136.2 %all-gather.11.cloned.1.call-start = ((), (), s32[]{:S(2)}) async-start(), calls=%async_computation.3 | async-start | bytes 2621440 | tf_op jit(solution)/shard_map/all_gather | solution.py:73
  9.8 198.1 %all-gather.13.cloned.1.call-start = ((), (), s32[]{:S(2)}) async-start(), calls=%async_computation.4 | async-start | bytes 6488064 | tf_op jit(solution)/shard_map/all_gather | solution.py:108
  10.4 290.0 %all-gather.15.cloned.1.call-start = ((), (), s32[]{:S(2)}) async-start(), calls=%async_computation.5 | async-start | bytes 6488064 | tf_op jit(solution)/shard_map/all_gather | solution.py:109
  11.0 382.7 %all-gather.17.cloned.1.call-start = ((), (), s32[]{:S(2)}) async-start(), calls=%async_computation.6 | async-start | bytes 6488064 | tf_op jit(solution)/shard_map/all_gather | solution.py:115
  11.6 419.8 %reduce-scatter.2.cloned.1.call-start = ((), (), s32[]{:S(2)}) async-start(), calls=%async_computation.7 | async-start | bytes 1966080 | tf_op jit(solution)/shard_map/reduce_scatter | solution.py:117
  50.4 0.8 copy-start.7
  50.4 1.5 copy-start.3
  85.8 1.8 copy-start.8
  85.8 9.7 %copy-start.4 = (bf16[384,128]{1,0:T(8,128)(2,1)S(1)}, bf16[384,128]{1,0:T(8,128)(2,1)}, u32[]{:S(2)}) copy-start(bf16[384,128]{1,0:T(8,128)(2,1)} %param.21) | copy-start | bytes 294916
  129.5 1.4 copy-start.1
  145.3 62.6 %copy-start.9 = (f32[2048]{0:T(1024)S(1)}, f32[2048]{0:T(1024)}, u32[]{:S(2)}) copy-start(f32[2048]{0:T(1024)} %param.26) | copy-start | bytes 24580
  207.9 185.8 %copy-start = (f32[384,2048]{1,0:T(8,128)S(1)}, f32[384,2048]{1,0:T(8,128)}, u32[]{:S(2)}) copy-start(f32[384,2048]{1,0:T(8,128)} %get-tuple-element.26) | copy-start | bytes 9437188
Sparse Core Ops, SparseCore 0:
  9.4 57.2 all-gather.8
  68.2 21.0 all-gather.6
  90.9 22.5 all-gather.10
  115.6 92.3 all-gather.12
  209.9 90.4 all-gather.14
  302.4 91.2 all-gather.16
  405.1 26.2 reduce-scatter.1
where the time goes:
time: 440 us
  waiting for transfers between devices  265 us (60%)
  blocking collectives  114 us (26%)
  matrix products  35.6 us (8%)
  between operations  13.7 us (3%)
  other arithmetic  7.87 us (2%)
    all_gather x1, waiting for transfers between devices, local(): lax.all_gather(w_down, 'sp', axis=1, tiled=True)  93.2 us
    all_gather x1, waiting for transfers between devices, local(): lax.all_gather(w_up, 'sp', axis=0, tiled=True)  84.8 us
    all_gather x1, waiting for transfers between devices, local(): lax.all_gather(w_gate, 'sp', axis=0, tiled=True)  57.6 us
    all_gather x1, blocking collectives, local(): lax.all_gather(keys_a, 'sp', axis=0, tiled=True)  35.7 us
    all_gather x1, blocking collectives, local(): lax.all_gather(values_a, 'sp', axis=0, tiled=True)  32.9 us
    all_gather x1, blocking collectives, local(): lax.all_gather(values_b, 'sp', axis=0, tiled=True)  32 us
    reduce_scatter x1, waiting for transfers between devices, local(): lax.psum_scatter(channel.astype(jnp.bfloat16), 'tp', scatter_dimension=1,...  26.4 us
    dot_general x1, matrix products, local(): jnp.dot(hidden, lax.all_gather(w_down, 'sp', axis=1, tiled=True), preferr...  11.2 us
  transfers between devices with their start and end apart: 7, of which 4 were waited for; matrix products, arithmetic and copies ran while one was open for 7% of the time, Pallas kernels for 0%

commit v1 on v0

v1 whole, which is shorter than its diff:
```python
import functools
import math

import jax
import jax.numpy as jnp
from jax import lax
from jax.experimental import pallas as pl
from jax.experimental.pallas import tpu as pltpu
from jax.sharding import PartitionSpec as P

eps_norm = 1e-06
head_scale = 0.8
MESH = pl.DeviceIdType.MESH
CHUNKS = 2
NT = (((1,), (1,)), ((), ()))


def ring_to_sp(pos, n):
    late = pos // (n // 2)
    return (1 - late) * 2 * pos + late * (2 * (n - 1 - pos) + 1)


def sp_to_ring(index, n):
    odd = index % 2
    return (1 - odd) * (index // 2) + odd * (n - 1 - (index - odd) // 2)


def kernel(
    n, tp, residual, qa, ka, va, qb, kb, vb, lam, gain, oa, ob, ngain, wg, wu, wd, out,
    kv_all, wg_all, wu_all, wd_all, out_all, heads_all, summed, normed, hidden, channel, sbuf, rbuf,
    mine, local_sem, ring_send, ring_recv, out_send, out_recv, head_send, head_recv, red_send, red_recv,
):
    rows, width = residual.shape
    heads = lam.shape[1]
    sa, sb = qa.shape[1] // (2 * heads), qb.shape[1] // (2 * heads)
    vd = va.shape[1] // heads
    hv = heads * vd
    block = math.gcd(rows, 128)
    nb = rows // block
    share = width // tp
    sp_me, tp_me = lax.axis_index("sp"), lax.axis_index("tp")
    pos = sp_to_ring(sp_me, n)
    targets = (ring_to_sp((pos + 1) % n, n), ring_to_sp((pos + n - 1) % n, n))
    peers = [(tp_me + k) % tp for k in range(1, tp)]

    ck, cv = ka.shape[1], ka.shape[1] + kb.shape[1]
    own_kv = kv_all.at[sp_me]
    own = [
        (ka, own_kv.at[:, pl.ds(0, ck)]),
        (kb, own_kv.at[:, pl.ds(ck, kb.shape[1])]),
        (va, own_kv.at[:, pl.ds(cv, hv)]),
        (vb, own_kv.at[:, pl.ds(cv + hv, hv)]),
        (wg, wg_all.at[sp_me]),
        (wu, wu_all.at[sp_me]),
        (wd, wd_all.at[sp_me]),
        (oa, out_all.at[tp_me, pl.ds(0, hv)]),
        (ob, out_all.at[tp_me, pl.ds(hv, hv)]),
    ]
    copies = [pltpu.make_async_copy(s, d, local_sem.at[i]) for i, (s, d) in enumerate(own)]
    for c in copies:
        c.start()

    barrier = pltpu.get_barrier_semaphore()
    for target in targets:
        pl.semaphore_signal(barrier, inc=1, device_id={"sp": target}, device_id_type=MESH)
    for peer in peers:
        pl.semaphore_signal(barrier, inc=1, device_id={"tp": peer}, device_id_type=MESH)
    for c in copies:
        c.wait()
    pl.semaphore_wait(barrier, 2 + len(peers))

    gathered = (kv_all, wg_all, wu_all, wd_all)

    def piece(a, c, d, t, dist):
        ref = gathered[a]
        owner = ring_to_sp((pos + n - dist) % n if d == 0 else (pos + dist) % n, n)
        part = ref.shape[1] // (2 * CHUNKS)
        view = ref.at[owner, pl.ds((d * CHUNKS + c) * part, part)]
        return pltpu.make_async_remote_copy(
            src_ref=view,
            dst_ref=view,
            send_sem=ring_send.at[a, c, d, t],
            recv_sem=ring_recv.at[a, c, d, t],
            device_id={"sp": targets[d]},
            device_id_type=MESH,
        )

    def begin(a):
        for c in range(CHUNKS):
            for d in range(2):
                piece(a, c, d, 0, 0).start()

    def step(a, c, t):
        for d in range(2):
            piece(a, c, d, t, t + 1).wait_recv()

            @pl.when(t + 1 < n - 1)
            def _():
                piece(a, c, d, t + 1, t + 1).start()

    def phase(a, work):
        def body(t, _):
            for c in range(CHUNKS):
                step(a, c, t)
                work(t * CHUNKS + c)
            return 0

        lax.fori_loop(0, n - 1, body, 0)

    slots = CHUNKS * (n - 1)

    begin(0)
    begin(1)

    def out_copy(k, target, slot):
        return pltpu.make_async_remote_copy(
            src_ref=out_all.at[slot], dst_ref=out_all.at[slot],
            send_sem=out_send.at[k], recv_sem=out_recv.at[k],
            device_id={"tp": target}, device_id_type=MESH,
        )

    def head_copy(k, target, slot):
        return pltpu.make_async_remote_copy(
            src_ref=mine, dst_ref=heads_all.at[slot],
            send_sem=head_send.at[k], recv_sem=head_recv.at[k],
            device_id={"tp": target}, device_id_type=MESH,
        )

    for k, peer in enumerate(peers):
        out_copy(k, peer, tp_me).start()

    phase(0, lambda slot: None)
    begin(2)

    total = n * rows

    def attend(group, r):
        queries = qa if group == 0 else qb
        size = sa if group == 0 else sb
        base = 0 if group == 0 else ck
        factor = size ** (-0.5) * math.log2(math.e)
        at = pl.ds(pl.multiple_of(r * block, block), block)
        for h in range(heads):
            start = 2 * h * size
            query = queries[at, start : start + 2 * size]
            value = kv_all[:, :, cv + group * hv + h * vd : cv + group * hv + (h + 1) * vd].reshape(total, vd)
            lanes = lax.broadcasted_iota(jnp.int32, query.shape, 1)
            ratios = []
            for j in range(2):
                if size % 128 == 0:
                    q = query[:, j * size : (j + 1) * size]
                    low = base + start + j * size
                    key = kv_all[:, :, low : low + size].reshape(total, size)
                else:
                    q = jnp.where(lanes // size == j, query, jnp.zeros_like(query))
                    low = base + start
                    key = kv_all[:, :, low : low + 2 * size].reshape(total, 2 * size)
                scores = lax.dot_general(q, key, NT, preferred_element_type=jnp.float32)
                peak = jnp.max(scores, axis=1, keepdims=True)
                weights = jnp.exp2((scores - peak) * factor)
                denom = jnp.sum(weights, axis=1, keepdims=True)
                numer = jnp.dot(weights.astype(jnp.bfloat16), value, preferred_element_type=jnp.float32)
                ratios.append(numer / denom)
            mixed = ratios[0] - lam[group, h] * ratios[1]
            inverse = lax.rsqrt(jnp.mean(mixed * mixed, axis=-1, keepdims=True) + eps_norm)
            result = mixed * inverse * gain[group : group + 1, :] * head_scale
            col = group * hv + h * vd
            mine[at, col : col + vd] = result.astype(jnp.bfloat16)

    def attend_slot(slot):
        @pl.when(slot < nb)
        def _():
            attend(0, slot)

        @pl.when((slot >= nb) & (slot < 2 * nb))
        def _():
            attend(1, slot - nb)

    phase(1, attend_slot)
    for slot in range(slots, 2 * nb):
        attend_slot(slot)
    begin(3)
    for k, peer in enumerate(peers):
        head_copy(k, peer, tp_me).start()

    def arrived():
        for k in range(tp - 1):
            source = (tp_me + tp - 1 - k) % tp
            head_copy(k, peers[k], source).wait_recv()
            out_copy(k, peers[k], source).wait_recv()
        heads_all[tp_me] = mine[...]

    def project(r):
        at = pl.ds(pl.multiple_of(r * block, block), block)
        acc = residual[at, :].astype(jnp.float32)
        for d in range(tp):
            acc = acc + jnp.dot(heads_all[d, at, :], out_all[d], preferred_element_type=jnp.float32)
        inverse = lax.rsqrt(jnp.mean(acc * acc, axis=-1, keepdims=True) + eps_norm)
        normed[at, :] = (acc * inverse * ngain[...]).astype(jnp.bfloat16)
        summed[at, :] = acc

    late = slots - nb

    def project_slot(slot):
        @pl.when(slot == late)
        def _():
            arrived()

        @pl.when(slot >= late)
        def _():
            project(slot - late)

    phase(2, project_slot)

    units = wg_all.shape[2]
    tile = math.gcd(units, 128)
    tiles = units // tile

    def feed(i):
        at = pl.ds(pl.multiple_of(i * tile, tile), tile)
        x = normed[...]
        gate = jnp.dot(x, wg_all[:, :, at].reshape(width, tile), preferred_element_type=jnp.float32)
        upward = jnp.dot(x, wu_all[:, :, at].reshape(width, tile), preferred_element_type=jnp.float32)
        hidden[:, at] = (gate / (1.0 + jnp.exp(-gate)) * upward).astype(jnp.bfloat16)

    per = -(-tiles // slots)

    def feed_slot(slot):
        for k in range(per):
            @pl.when(slot * per + k < tiles)
            def _():
                feed(slot * per + k)

    phase(3, feed_slot)

    cols = wd_all.shape[2]
    ratio = share // cols
    for d in range(tp):
        for s in range(ratio):
            channel[d, :, s * cols : (s + 1) * cols] = jnp.dot(
                hidden[...], wd_all[d * ratio + s], preferred_element_type=jnp.float32
            )

    bit, used, pending = 1, 0, []
    while bit < tp:
        flag = (tp_me // bit) % 2
        partner = tp_me + bit - 2 * bit * flag
        count = tp // (2 * bit)
        batch = []
        for m in range(count):
            give = tp_me % bit + bit * (1 - flag) + 2 * bit * m
            keep = tp_me % bit + bit * flag + 2 * bit * m
            sbuf[give] = channel[give].astype(jnp.bfloat16)
            copy = pltpu.make_async_remote_copy(
                src_ref=sbuf.at[give], dst_ref=rbuf.at[used],
                send_sem=red_send.at[used], recv_sem=red_recv.at[used],
                device_id={"tp": partner}, device_id_type=MESH,
            )
            copy.start()
            batch.append((copy, keep, used))
            used += 1
        for copy, keep, slot in batch:
            copy.wait_recv()
            channel[keep] = channel[keep] + rbuf[slot].astype(jnp.float32)
            pending.append(copy)
        bit *= 2

    at = pl.ds(pl.multiple_of(tp_me * share, share), share)
    out[...] = (summed[:, at] + 0.5 * channel[tp_me]).astype(jnp.bfloat16)

    for copy in pending:
        copy.wait_send()
    for k, peer in enumerate(peers):
        out_copy(k, peer, tp_me).wait_send()
        head_copy(k, peer, tp_me).wait_send()

    def drain(t, _):
        for a in range(len(gathered)):
            for c in range(CHUNKS):
                for d in range(2):
                    piece(a, c, d, t, t).wait_send()
        return 0

    lax.fori_loop(0, n - 1, drain, 0)


def local(
    n, tp, residual, queries_a, keys_a, values_a, queries_b, keys_b, values_b, mix_lambda, head_gain,
    out_a, out_b, norm_gain, w_gate, w_up, w_down,
):
    rows, width = residual.shape
    share = width // tp
    units = w_gate.shape[1]
    hv = out_a.shape[0]
    span = keys_a.shape[1] + keys_b.shape[1] + values_a.shape[1] + values_b.shape[1]
    vmem, anywhere = pl.BlockSpec(memory_space=pltpu.VMEM), pl.BlockSpec(memory_space=pl.ANY)
    smem = pl.BlockSpec(memory_space=pltpu.SMEM)
    bf16, f32 = jnp.bfloat16, jnp.float32
    dma = pltpu.SemaphoreType.DMA
    return pl.pallas_call(
        functools.partial(kernel, n, tp),
        out_shape=jax.ShapeDtypeStruct((rows, share), bf16),
        in_specs=[
            vmem, vmem, anywhere, anywhere, vmem, anywhere, anywhere, smem, vmem,
            anywhere, anywhere, vmem, anywhere, anywhere, anywhere,
        ],
        out_specs=vmem,
        scratch_shapes=[
            pltpu.VMEM((n, rows, span), bf16),
            pltpu.VMEM((n,) + w_gate.shape, bf16),
            pltpu.VMEM((n,) + w_up.shape, bf16),
            pltpu.VMEM((n,) + w_down.shape, bf16),
            pltpu.VMEM((tp, 2 * hv, width), bf16),
            pltpu.VMEM((tp, rows, 2 * hv), bf16),
            pltpu.VMEM((rows, width), f32),
            pltpu.VMEM((rows, width), bf16),
            pltpu.VMEM((rows, units), bf16),
            pltpu.VMEM((tp, rows, share), f32),
            pltpu.VMEM((tp, rows, share), bf16),
            pltpu.VMEM((tp - 1, rows, share), bf16),
            pltpu.VMEM((rows, 2 * hv), bf16),
            dma((9,)),
            dma((4, CHUNKS, 2, n - 1)),
            dma((4, CHUNKS, 2, n - 1)),
            dma((tp - 1,)),
            dma((tp - 1,)),
            dma((tp - 1,)),
            dma((tp - 1,)),
            dma((tp - 1,)),
            dma((tp - 1,)),
        ],
        compiler_params=pltpu.CompilerParams(
            collective_id=0, has_side_effects=True, vmem_limit_bytes=63 * 1024 * 1024
        ),
        name="layer",
    )(
        residual, queries_a, keys_a, values_a, queries_b, keys_b, values_b, mix_lambda, head_gain,
        out_a, out_b, norm_gain.reshape(1, -1), w_gate, w_up, w_down,
    )


def solution(mesh):
    in_specs = (
        P("sp", None),
        P("sp", "tp"),
        P("sp", "tp"),
        P("sp", "tp"),
        P("sp", "tp"),
        P("sp", "tp"),
        P("sp", "tp"),
        P(None, "tp"),
        P(),
        P("tp", None),
        P("tp", None),
        P(),
        P("sp", "tp"),
        P("sp", "tp"),
        P("tp", "sp"),
    )
    body = functools.partial(local, mesh.shape["sp"], mesh.shape["tp"])
    return jax.shard_map(body, mesh=mesh, in_specs=in_specs, out_specs=P("sp", "tp"), check_vma=False)
```

time: 440 us -> 231 us (0.53)
  waiting for transfers between devices: 265 us -> 0 us
  Pallas kernels: 0 us -> 227 us
  blocking collectives: 114 us -> 0 us
  matrix products: 35.6 us -> 0 us
  between operations: 13.7 us -> 0.01 us
  other arithmetic: 7.87 us -> 0 us
    all_gather x6 -> x0, waiting for transfers between devices: 236 us -> none  [the longest x1 93.2 us: local(): lax.all_gather(w_down, 'sp', axis=1, tiled=True)]
    pallas_call x0 -> x1, Pallas kernels: none -> 227 us  [local(): pl.pallas_call(functools.partial(kernel, n, tp), out_shape=jax.ShapeDtype...]
    all_gather x5 -> x0, blocking collectives: 114 us -> none  [the longest x1 35.7 us: local(): lax.all_gather(keys_a, 'sp', axis=0, tiled=True)]
    dot_general x12 -> x0, matrix products: 35.6 us -> none  [the longest x1 11.2 us: local(): jnp.dot(hidden, lax.all_gather(w_down, 'sp', axis=1, tiled=True), preferr...]
    reduce_scatter x1 -> x0, waiting for transfers between devices: 26.4 us -> none  [local(): lax.psum_scatter(channel.astype(jnp.bfloat16), 'tp', scatter_dimension=1,...]
    reduce_sum x6 -> x0, other arithmetic: 4.45 us -> none  [the longest x4 3.11 us: group_update(): denoms.append(denom[which] * decay + jnp.sum(weights, axis=-1))]
  transfers between devices with their start and end apart: 7 -> 0, of which waited for: 4 -> 0; matrix products, arithmetic and copies ran while one was open for 7% -> 0% of each run, Pallas kernels for 0% -> 0%
where the time goes in v1:
time: 231 us; the launch traced here: 230 us
  Pallas kernels  227 us (98%)
  local copies, waits for them, and re-layouts  3.06 us (1%)
    pallas_call x1, Pallas kernels, local(): pl.pallas_call(functools.partial(kernel, n, tp), out_shape=jax.ShapeDtype...  227 us

profile of v1, /device:TPU:0, one launch (start us, length us, event | category | flops | bytes accessed | tf_op | source)
XLA Modules:
  0.0 230.0 jit_solution(15659853579353061520)
XLA Ops:
  0.0 1.3 copy.16.lam
  1.3 226.9 %layer.1 = bf16[384,512]{1,0:T(8,128)(2,1)} custom-call(bf16[384,2048]{1,0:T(8,128)(2,1)} %residual.1, bf16[384,128]{1,0:T(8,128)(2,1)} %qa.1, bf16[384,128]{1,0:T(8,128)(2,1)} %ka.1, bf16[384,128]{1,0:T(8,128)(2,1)} %va.1, bf16[384,256]{1,0:T(8,128)(2,1)} %qb.1, bf16[384,256]{1,0:T(8,128)(2,1)} %kb.1, bf16[384,128]{1,0:T(8,128)(2,1)} %vb.1, ...), custom_call_target="tpu_custom_call" | custom-call | tf_op jit(solution)/shard_map/layer/pallas_call | solution.py:300
  228.2 1.8 copy.18

commit v2 on v1

v2 whole, which is shorter than its diff:
```python
import functools
import math

import jax
import jax.numpy as jnp
from jax import lax
from jax.experimental import pallas as pl
from jax.experimental.pallas import tpu as pltpu
from jax.sharding import PartitionSpec as P

eps_norm = 1e-06
head_scale = 0.8
MESH = pl.DeviceIdType.MESH
CHUNKS = 2
CUTS = 3
NT = (((1,), (1,)), ((), ()))


def ring_to_sp(pos, n):
    late = pos // (n // 2)
    return (1 - late) * 2 * pos + late * (2 * (n - 1 - pos) + 1)


def sp_to_ring(index, n):
    odd = index % 2
    return (1 - odd) * (index // 2) + odd * (n - 1 - (index - odd) // 2)


def flip(index, bit):
    return index + bit - 2 * bit * ((index // bit) % 2)


def flip_all(index, mask):
    bit = 1
    while bit <= mask:
        if mask & bit:
            index = flip(index, bit)
        bit *= 2
    return index


def kernel(
    n, tp, residual, qa, ka, va, qb, kb, vb, lam, gain, oa, ob, ngain, wg, wu, wd, out,
    kv_all, wg_turn, wu_turn, wg_all, wu_all, wd_all, out_all, heads_all, summed, normed, hidden, channel, sbuf,
    rbuf, tbuf, mine, local_sem, ring_send, ring_recv, cube_send, cube_recv, out_send, out_recv, head_send,
    head_recv, norm_send, norm_recv, red_send, red_recv,
):
    rows, width = residual.shape
    heads = lam.shape[1]
    sa, sb = qa.shape[1] // (2 * heads), qb.shape[1] // (2 * heads)
    vd = va.shape[1] // heads
    hv = heads * vd
    total = n * rows
    block = math.gcd(rows, 1 << min(7, ((1 << 19) // total).bit_length() - 1))
    nb = rows // block
    share = width // tp
    depth, units = wg.shape
    half = units // 2
    sp_me, tp_me = lax.axis_index("sp"), lax.axis_index("tp")
    pos = sp_to_ring(sp_me, n)
    targets = (ring_to_sp((pos + 1) % n, n), ring_to_sp((pos + n - 1) % n, n))
    peers = [(tp_me + k) % tp for k in range(1, tp)]
    pair = n // 4
    side = (sp_me // pair) % 2
    mate = flip(sp_me, pair)
    bits = [pair, n // 2]
    while bits[-1 if len(bits) > 2 else 0] > 1:
        bits.append(bits[-1] // 2 if len(bits) > 2 else pair // 2)

    ck, cv = ka.shape[1], ka.shape[1] + kb.shape[1]
    own_kv = kv_all.at[sp_me]
    own = [
        (ka, own_kv.at[:, pl.ds(0, ck)]),
        (kb, own_kv.at[:, pl.ds(ck, kb.shape[1])]),
        (va, own_kv.at[:, pl.ds(cv, hv)]),
        (vb, own_kv.at[:, pl.ds(cv + hv, hv)]),
        (wd.at[pl.ds(pl.multiple_of(side * half, half), half)], wd_all.at[sp_me]),
        (oa, out_all.at[tp_me, pl.ds(0, hv)]),
        (ob, out_all.at[tp_me, pl.ds(hv, hv)]),
    ]
    copies = [pltpu.make_async_copy(s, d, local_sem.at[i]) for i, (s, d) in enumerate(own)]
    for c in copies:
        c.start()

    barrier = pltpu.get_barrier_semaphore()
    for target in list(targets) + [flip(sp_me, bit) for bit in bits]:
        pl.semaphore_signal(barrier, inc=1, device_id={"sp": target}, device_id_type=MESH)
    for peer in peers:
        pl.semaphore_signal(barrier, inc=1, device_id={"tp": peer}, device_id_type=MESH)
    for c in copies:
        c.wait()
    pl.semaphore_wait(barrier, 2 + len(bits) + len(peers))

    def piece(c, d, t, dist):
        owner = ring_to_sp((pos + n - dist) % n if d == 0 else (pos + dist) % n, n)
        part = rows // (2 * CHUNKS)
        view = kv_all.at[owner, pl.ds((d * CHUNKS + c) * part, part)]
        return pltpu.make_async_remote_copy(
            src_ref=view, dst_ref=view,
            send_sem=ring_send.at[c, d, t], recv_sem=ring_recv.at[c, d, t],
            device_id={"sp": targets[d]}, device_id_type=MESH,
        )

    for c in range(CHUNKS):
        for d in range(2):
            piece(c, d, 0, 0).start()

    def out_copy(k, target, slot):
        return pltpu.make_async_remote_copy(
            src_ref=out_all.at[slot], dst_ref=out_all.at[slot],
            send_sem=out_send.at[k], recv_sem=out_recv.at[k],
            device_id={"tp": target}, device_id_type=MESH,
        )

    def head_copy(k, target, slot):
        return pltpu.make_async_remote_copy(
            src_ref=mine, dst_ref=heads_all.at[slot],
            send_sem=head_send.at[k], recv_sem=head_recv.at[k],
            device_id={"tp": target}, device_id_type=MESH,
        )

    for k, peer in enumerate(peers):
        out_copy(k, peer, tp_me).start()

    tile = math.gcd(units, 128)

    def turn(i):
        at = pl.ds(pl.multiple_of(i * tile, tile), tile)
        wg_turn[at, :] = wg[:, at].T
        wu_turn[at, :] = wu[:, at].T

    turns = units // tile
    per = -(-turns // (n - 1))

    def circulate(t, _):
        for c in range(CHUNKS):
            for d in range(2):
                piece(c, d, t, t + 1).wait_recv()

                @pl.when(t + 1 < n - 1)
                def _():
                    piece(c, d, t + 1, t + 1).start()

        for k in range(per):
            @pl.when(t * per + k < turns)
            def _():
                turn(t * per + k)

        return 0

    lax.fori_loop(0, n - 1, circulate, 0)
    wg_all[sp_me] = wg_turn[pl.ds(pl.multiple_of(side * half, half), half), :]
    wu_all[sp_me] = wu_turn[pl.ds(pl.multiple_of(side * half, half), half), :]

    gathered = (wg_all, wu_all, wd_all)
    whole = (wg_turn, wu_turn, wd)

    def cube(a, held, k, arriving):
        mask = held | bits[k]
        owner = flip_all(sp_me, mask if arriving else held)
        dst = gathered[a].at[owner]
        src = dst
        if k == 0 and not arriving:
            src = whole[a].at[pl.ds(pl.multiple_of((1 - side) * half, half), half)]
        return pltpu.make_async_remote_copy(
            src_ref=src, dst_ref=dst,
            send_sem=cube_send.at[a, mask], recv_sem=cube_recv.at[a, mask],
            device_id={"sp": flip(sp_me, bits[k])}, device_id_type=MESH,
        )

    order = [0]
    came = {}
    for k, bit in enumerate(bits):
        for held in list(order):
            came[held | bit] = (held, k)
            order.append(held | bit)

    def forward(a, mask):
        first = came[mask][1] + 1 if mask else 0
        for k in range(first, len(bits)):
            cube(a, mask, k, False).start()

    def arrive(a, mask):
        held, k = came[mask]
        cube(a, held, k, True).wait_recv()
        forward(a, mask)

    for a in range(3):
        forward(a, 0)
    events = []
    for k in range(len(bits)):
        for a in range(3):
            for mask in order[1:]:
                if came[mask][1] == k:
                    events.append((a, mask))

    def take(count):
        for a, mask in events[:count]:
            arrive(a, mask)
        del events[:count]

    def attend(group, r):
        queries = qa if group == 0 else qb
        size = sa if group == 0 else sb
        base = 0 if group == 0 else ck
        factor = size ** (-0.5) * math.log2(math.e)
        at = pl.ds(pl.multiple_of(r * block, block), block)
        for h in range(heads):
            start = 2 * h * size
            query = queries[at, start : start + 2 * size]
            value = kv_all[:, :, cv + group * hv + h * vd : cv + group * hv + (h + 1) * vd].reshape(total, vd)
            lanes = lax.broadcasted_iota(jnp.int32, query.shape, 1)
            ratios = []
            for j in range(2):
                if size % 128 == 0:
                    q = query[:, j * size : (j + 1) * size]
                    low = base + start + j * size
                    key = kv_all[:, :, low : low + size].reshape(total, size)
                else:
                    q = jnp.where(lanes // size == j, query, jnp.zeros_like(query))
                    low = base + start
                    key = kv_all[:, :, low : low + 2 * size].reshape(total, 2 * size)
                scores = lax.dot_general(q, key, NT, preferred_element_type=jnp.float32)
                peak = jnp.max(scores, axis=1, keepdims=True)
                weights = jnp.exp2((scores - peak) * factor)
                denom = jnp.sum(weights, axis=1, keepdims=True)
                numer = jnp.dot(weights.astype(jnp.bfloat16), value, preferred_element_type=jnp.float32)
                ratios.append(numer / denom)
            mixed = ratios[0] - lam[group, h] * ratios[1]
            inverse = lax.rsqrt(jnp.mean(mixed * mixed, axis=-1, keepdims=True) + eps_norm)
            result = mixed * inverse * gain[group : group + 1, :] * head_scale
            col = group * hv + h * vd
            mine[at, col : col + vd] = result.astype(jnp.bfloat16)

    early = sum(1 for _, mask in events if came[mask][1] < 2)
    portion = -(-early // (2 * CUTS))
    cuts = [nb * i // CUTS for i in range(CUTS + 1)]
    for group in range(2):
        for i in range(CUTS):
            def body(r, _, group=group):
                attend(group, r)
                return 0

            lax.fori_loop(cuts[i], cuts[i + 1], body, 0)
            take(min(portion, early))
            early -= min(portion, early)

    for k, peer in enumerate(peers):
        head_copy(k, peer, tp_me).start()
    for k in range(tp - 1):
        source = (tp_me + tp - 1 - k) % tp
        head_copy(k, peers[k], source).wait_recv()
        out_copy(k, peers[k], source).wait_recv()
    heads_all[tp_me] = mine[...]

    def project(r, _):
        at = pl.ds(pl.multiple_of(r * block, block), block)
        acc = residual[at, :].astype(jnp.float32)
        for d in range(tp):
            acc = acc + jnp.dot(heads_all[d, at, :], out_all[d], preferred_element_type=jnp.float32)
        inverse = lax.rsqrt(jnp.mean(acc * acc, axis=-1, keepdims=True) + eps_norm)
        scaled = (acc * inverse * ngain[...]).astype(jnp.bfloat16)
        for d in range(tp):
            normed[side, d, at, :] = scaled[:, d * share : (d + 1) * share]
            summed[d, at, :] = acc[:, d * share : (d + 1) * share].astype(summed.dtype)
        return 0

    lax.fori_loop(0, nb, project, 0)

    def swap(arriving):
        there = 1 - side if arriving else side
        view = normed.at[there, tp_me]
        return pltpu.make_async_remote_copy(
            src_ref=view, dst_ref=view, send_sem=norm_send.at[0], recv_sem=norm_recv.at[0],
            device_id={"sp": mate}, device_id_type=MESH,
        )

    def spread(k, target, slot):
        view = normed.at[1 - side, slot]
        return pltpu.make_async_remote_copy(
            src_ref=view, dst_ref=view, send_sem=norm_send.at[1 + k], recv_sem=norm_recv.at[1 + k],
            device_id={"tp": target}, device_id_type=MESH,
        )

    swap(False).start()
    take(sum(1 for a, _ in events if a == 0))
    swap(True).wait_recv()
    for k, peer in enumerate(peers):
        spread(k, peer, tp_me).start()
    take(sum(1 for a, _ in events if a == 1))

    step_cols = share // depth

    def feed(where):
        gate = jnp.zeros((rows, half), jnp.float32)
        upward = jnp.zeros((rows, half), jnp.float32)
        for s in range(n):
            low = (s % step_cols) * depth
            x = normed[where, s // step_cols, :, low : low + depth]
            gate = gate + lax.dot_general(x, wg_all[s], NT, preferred_element_type=jnp.float32)
            upward = upward + lax.dot_general(x, wu_all[s], NT, preferred_element_type=jnp.float32)
        hidden[where] = (gate / (1.0 + jnp.exp(-gate)) * upward).astype(jnp.bfloat16)

    def feed_one(i, _):
        @pl.when(i == 1)
        def _():
            for k in range(tp - 1):
                spread(k, peers[k], (tp_me + tp - 1 - k) % tp).wait_recv()

        feed((side + i) % 2)
        return 0

    lax.fori_loop(0, 2, feed_one, 0)
    take(len(events))

    cols = wd_all.shape[2]
    ratio = share // cols
    low_bit = tp_me % 2

    def block_sum(d, where):
        return [
            jnp.dot(hidden[where], wd_all[d * ratio + s], preferred_element_type=jnp.float32)
            for s in range(ratio)
        ]

    used, pending = 0, []

    def send(src, **target):
        nonlocal used
        copy = pltpu.make_async_remote_copy(
            src_ref=src, dst_ref=rbuf.at[used], send_sem=red_send.at[used], recv_sem=red_recv.at[used],
            device_id=target, device_id_type=MESH,
        )
        copy.start()
        pending.append(copy)
        used += 1

    for i in range(2):
        for m in range(tp // 2):
            d = 2 * m + (1 - low_bit if i == 0 else low_bit)
            for where in range(2):
                for s, value in enumerate(block_sum(d, where)):
                    if i == 0:
                        sbuf[2 * m + where, :, s * cols : (s + 1) * cols] = value.astype(jnp.bfloat16)
                    else:
                        channel[2 * m + where, :, s * cols : (s + 1) * cols] = value
                if i == 0:
                    send(sbuf.at[2 * m + where], tp=flip(tp_me, 1))
    for m in range(tp):
        pending[m].wait_recv()
        channel[m] = channel[m] + rbuf[m].astype(jnp.float32)

    bit, sent = 2, 0
    while bit < tp:
        flag = (tp_me // bit) % 2
        count = tp // (2 * bit)
        batch = []
        for m in range(count):
            give = (tp_me % bit + bit * (1 - flag) + 2 * bit * m) // 2
            keep = (tp_me % bit + bit * flag + 2 * bit * m) // 2
            for i in range(2):
                where = (1 - side) if i == 0 else side
                tbuf[sent] = channel[2 * give + where].astype(jnp.bfloat16)
                batch.append((used, 2 * keep + where))
                send(tbuf.at[sent], tp=flip(tp_me, bit))
                sent += 1
        for slot, keep in batch:
            pending[slot].wait_recv()
            channel[keep] = channel[keep] + rbuf[slot].astype(jnp.float32)
        bit *= 2
    tbuf[sent] = channel[2 * (tp_me // 2) + 1 - side].astype(jnp.bfloat16)
    last = used
    send(tbuf.at[sent], sp=mate)
    pending[last].wait_recv()
    final = channel[2 * (tp_me // 2) + side] + rbuf[last].astype(jnp.float32)
    out[...] = (summed[tp_me] + 0.5 * final).astype(jnp.bfloat16)

    for copy in pending:
        copy.wait_send()
    swap(False).wait_send()
    for k, peer in enumerate(peers):
        out_copy(k, peer, tp_me).wait_send()
        head_copy(k, peer, tp_me).wait_send()
        spread(k, peer, tp_me).wait_send()
    for a in range(3):
        for mask in order[1:]:
            held, k = came[mask]
            cube(a, held, k, False).wait_send()

    def drain(t, _):
        for c in range(CHUNKS):
            for d in range(2):
                piece(c, d, t, t).wait_send()
        return 0

    lax.fori_loop(0, n - 1, drain, 0)


def local(
    n, tp, residual, queries_a, keys_a, values_a, queries_b, keys_b, values_b, mix_lambda, head_gain,
    out_a, out_b, norm_gain, w_gate, w_up, w_down,
):
    rows, width = residual.shape
    share = width // tp
    units = w_gate.shape[1]
    hv = out_a.shape[0]
    span = keys_a.shape[1] + keys_b.shape[1] + values_a.shape[1] + values_b.shape[1]
    vmem, anywhere = pl.BlockSpec(memory_space=pltpu.VMEM), pl.BlockSpec(memory_space=pl.ANY)
    smem = pl.BlockSpec(memory_space=pltpu.SMEM)
    bf16, f32 = jnp.bfloat16, jnp.float32
    dma = pltpu.SemaphoreType.DMA
    return pl.pallas_call(
        functools.partial(kernel, n, tp),
        out_shape=jax.ShapeDtypeStruct((rows, share), bf16),
        in_specs=[
            vmem, vmem, anywhere, anywhere, vmem, anywhere, anywhere, smem, vmem,
            anywhere, anywhere, vmem, vmem, vmem, anywhere,
        ],
        out_specs=vmem,
        scratch_shapes=[
            pltpu.VMEM((n, rows, span), bf16),
            pltpu.VMEM((units, w_gate.shape[0]), bf16),
            pltpu.VMEM((units, w_gate.shape[0]), bf16),
            pltpu.VMEM((n, units // 2, w_gate.shape[0]), bf16),
            pltpu.VMEM((n, units // 2, w_gate.shape[0]), bf16),
            pltpu.VMEM((n, units // 2, w_down.shape[1]), bf16),
            pltpu.VMEM((tp, 2 * hv, width), bf16),
            pltpu.VMEM((tp, rows, 2 * hv), bf16),
            pltpu.VMEM((tp, rows, share), f32),
            pltpu.VMEM((2, tp, rows, share), bf16),
            pltpu.VMEM((2, rows, units // 2), bf16),
            pltpu.VMEM((tp, rows, share), f32),
            pltpu.VMEM((tp, rows, share), bf16),
            pltpu.VMEM((2 * tp - 1, rows, share), bf16),
            pltpu.VMEM((tp - 1, rows, share), bf16),
            pltpu.VMEM((rows, 2 * hv), bf16),
            dma((7,)),
            dma((CHUNKS, 2, n - 1)),
            dma((CHUNKS, 2, n - 1)),
            dma((3, n)),
            dma((3, n)),
            dma((tp - 1,)),
            dma((tp - 1,)),
            dma((tp - 1,)),
            dma((tp - 1,)),
            dma((tp,)),
            dma((tp,)),
            dma((2 * tp - 1,)),
            dma((2 * tp - 1,)),
        ],
        compiler_params=pltpu.CompilerParams(
            collective_id=0, has_side_effects=True, vmem_limit_bytes=63 * 1024 * 1024
        ),
        name="layer",
    )(
        residual, queries_a, keys_a, values_a, queries_b, keys_b, values_b, mix_lambda, head_gain,
        out_a, out_b, norm_gain.reshape(1, -1), w_gate, w_up, w_down,
    )


def solution(mesh):
    in_specs = (
        P("sp", None),
        P("sp", "tp"),
        P("sp", "tp"),
        P("sp", "tp"),
        P("sp", "tp"),
        P("sp", "tp"),
        P("sp", "tp"),
        P(None, "tp"),
        P(),
        P("tp", None),
        P("tp", None),
        P(),
        P("sp", "tp"),
        P("sp", "tp"),
        P("tp", "sp"),
    )
    body = functools.partial(local, mesh.shape["sp"], mesh.shape["tp"])
    return jax.shard_map(body, mesh=mesh, in_specs=in_specs, out_specs=P("sp", "tp"), check_vma=False)
```

time: 231 us -> 220 us (0.952)
  Pallas kernels: 227 us -> 217 us
    pallas_call x1, Pallas kernels: 227 us -> 217 us  [local(): pl.pallas_call(functools.partial(kernel, n, tp), out_shape=jax.ShapeDtype...]
where the time goes in v2:
time: 220 us
  Pallas kernels  217 us (99%)
  local copies, waits for them, and re-layouts  3.06 us (1%)
    pallas_call x1, Pallas kernels, local(): pl.pallas_call(functools.partial(kernel, n, tp), out_shape=jax.ShapeDtype...  217 us

profile of v2, /device:TPU:0, one launch (start us, length us, event | category | flops | bytes accessed | tf_op | source)
XLA Modules:
  0.0 220.0 jit_solution(11033112122620573315)
XLA Ops:
  0.0 1.3 copy.16.lam
  1.3 216.9 %layer.1 = bf16[384,512]{1,0:T(8,128)(2,1)} custom-call(bf16[384,2048]{1,0:T(8,128)(2,1)} %residual.1, bf16[384,128]{1,0:T(8,128)(2,1)} %qa.1, bf16[384,128]{1,0:T(8,128)(2,1)} %ka.1, bf16[384,128]{1,0:T(8,128)(2,1)} %va.1, bf16[384,256]{1,0:T(8,128)(2,1)} %qb.1, bf16[384,256]{1,0:T(8,128)(2,1)} %kb.1, bf16[384,128]{1,0:T(8,128)(2,1)} %vb.1, ...), custom_call_target="tpu_custom_call" | custom-call | tf_op jit(solution)/shard_map/layer/pallas_call | solution.py:412
  218.2 1.8 copy.18

commit v3 on v2

--- a/solution.py
+++ b/solution.py
@@ -42,8 +42,8 @@
 def kernel(
     n, tp, residual, qa, ka, va, qb, kb, vb, lam, gain, oa, ob, ngain, wg, wu, wd, out,
     kv_all, wg_turn, wu_turn, wg_all, wu_all, wd_all, out_all, heads_all, summed, normed, hidden, channel, sbuf,
-    rbuf, tbuf, mine, local_sem, ring_send, ring_recv, cube_send, cube_recv, out_send, out_recv, head_send,
-    head_recv, norm_send, norm_recv, red_send, red_recv,
+    rbuf, tbuf, ubuf, mine, local_sem, ring_send, ring_recv, cube_send, cube_recv, out_send, out_recv, head_send,
+    head_recv, swap_sem, norm_send, norm_recv, red_send, red_recv,
 ):
     rows, width = residual.shape
     heads = lam.shape[1]
@@ -105,22 +105,44 @@
         for d in range(2):
             piece(c, d, 0, 0).start()
 
-    def out_copy(k, target, slot):
+    tp_bits = []
+    while (tp >> (len(tp_bits) + 1)) > 0:
+        tp_bits.append(tp >> (len(tp_bits) + 1))
+    tp_order, tp_came = [0], {}
+    for k, bit in enumerate(tp_bits):
+        for held in list(tp_order):
+            tp_came[held | bit] = (held, k)
+            tp_order.append(held | bit)
+
+    def tp_copy(gather, held, k, arriving):
+        view, first, sends, recvs = gather
+        mask = held | tp_bits[k]
+        dst = view(flip_all(tp_me, mask if arriving else held))
         return pltpu.make_async_remote_copy(
-            src_ref=out_all.at[slot], dst_ref=out_all.at[slot],
-            send_sem=out_send.at[k], recv_sem=out_recv.at[k],
-            device_id={"tp": target}, device_id_type=MESH,
+            src_ref=first if first is not None and held == 0 and not arriving else dst, dst_ref=dst,
+            send_sem=sends.at[mask - 1], recv_sem=recvs.at[mask - 1],
+            device_id={"tp": flip(tp_me, tp_bits[k])}, device_id_type=MESH,
         )
 
-    def head_copy(k, target, slot):
-        return pltpu.make_async_remote_copy(
-            src_ref=mine, dst_ref=heads_all.at[slot],
-            send_sem=head_send.at[k], recv_sem=head_recv.at[k],
-            device_id={"tp": target}, device_id_type=MESH,
-        )
-
-    for k, peer in enumerate(peers):
-        out_copy(k, peer, tp_me).start()
+    def tp_forward(gather, mask):
+        for k in range(tp_came[mask][1] + 1 if mask else 0, len(tp_bits)):
+            tp_copy(gather, mask, k, False).start()
+
+    def tp_arrive(gather, masks):
+        for mask in masks:
+            held, k = tp_came[mask]
+            tp_copy(gather, held, k, True).wait_recv()
+            tp_forward(gather, mask)
+
+    def tp_drain(gather):
+        for mask in tp_order[1:]:
+            held, k = tp_came[mask]
+            tp_copy(gather, held, k, False).wait_send()
+
+    out_gather = (lambda slot: out_all.at[slot], None, out_send, out_recv)
+    head_gather = (lambda slot: heads_all.at[slot], mine, head_send, head_recv)
+    norm_gather = (lambda slot: normed.at[1 - side, slot], None, norm_send, norm_recv)
+    tp_forward(out_gather, 0)
 
     tile = math.gcd(units, 128)
 
@@ -175,9 +197,9 @@
             came[held | bit] = (held, k)
             order.append(held | bit)
 
-    def forward(a, mask):
+    def forward(a, mask, least=0, most=len(bits)):
         first = came[mask][1] + 1 if mask else 0
-        for k in range(first, len(bits)):
+        for k in range(max(first, least), most):
             cube(a, mask, k, False).start()
 
     def arrive(a, mask):
@@ -185,8 +207,9 @@
         cube(a, held, k, True).wait_recv()
         forward(a, mask)
 
-    for a in range(3):
-        forward(a, 0)
+    forward(0, 0)
+    forward(1, 0)
+    forward(2, 0, least=2)
     events = []
     for k in range(len(bits)):
         for a in range(3):
@@ -194,10 +217,10 @@
                 if came[mask][1] == k:
                     events.append((a, mask))
 
-    def take(count):
-        for a, mask in events[:count]:
+    def take(chosen):
+        for a, mask in chosen:
             arrive(a, mask)
-        del events[:count]
+            events.remove((a, mask))
 
     def attend(group, r):
         queries = qa if group == 0 else qb
@@ -232,8 +255,8 @@
             col = group * hv + h * vd
             mine[at, col : col + vd] = result.astype(jnp.bfloat16)
 
-    early = sum(1 for _, mask in events if came[mask][1] < 2)
-    portion = -(-early // (2 * CUTS))
+    early = [(a, mask) for a, mask in events if a < 2 and came[mask][1] < 2]
+    portion = -(-len(early) // (2 * CUTS))
     cuts = [nb * i // CUTS for i in range(CUTS + 1)]
     for group in range(2):
         for i in range(CUTS):
@@ -242,15 +265,15 @@
                 return 0
 
             lax.fori_loop(cuts[i], cuts[i + 1], body, 0)
-            take(min(portion, early))
-            early -= min(portion, early)
-
-    for k, peer in enumerate(peers):
-        head_copy(k, peer, tp_me).start()
-    for k in range(tp - 1):
-        source = (tp_me + tp - 1 - k) % tp
-        head_copy(k, peers[k], source).wait_recv()
-        out_copy(k, peers[k], source).wait_recv()
+            take(early[:portion])
+            early = early[portion:]
+            if group == 0 and i == 0:
+                tp_arrive(out_gather, tp_order[1:-1])
+            if group == 0 and i == 1:
+                tp_arrive(out_gather, tp_order[-1:])
+
+    tp_forward(head_gather, 0)
+    tp_arrive(head_gather, tp_order[1:])
     heads_all[tp_me] = mine[...]
 
     def project(r, _):
@@ -271,23 +294,17 @@
         there = 1 - side if arriving else side
         view = normed.at[there, tp_me]
         return pltpu.make_async_remote_copy(
-            src_ref=view, dst_ref=view, send_sem=norm_send.at[0], recv_sem=norm_recv.at[0],
+            src_ref=view, dst_ref=view, send_sem=swap_sem.at[0], recv_sem=swap_sem.at[1],
             device_id={"sp": mate}, device_id_type=MESH,
         )
 
-    def spread(k, target, slot):
-        view = normed.at[1 - side, slot]
-        return pltpu.make_async_remote_copy(
-            src_ref=view, dst_ref=view, send_sem=norm_send.at[1 + k], recv_sem=norm_recv.at[1 + k],
-            device_id={"tp": target}, device_id_type=MESH,
-        )
-
     swap(False).start()
-    take(sum(1 for a, _ in events if a == 0))
+    forward(2, 0, most=2)
+    take([e for e in events if e[0] == 2 and came[e[1]][1] == 0])
     swap(True).wait_recv()
-    for k, peer in enumerate(peers):
-        spread(k, peer, tp_me).start()
-    take(sum(1 for a, _ in events if a == 1))
+    tp_forward(norm_gather, 0)
+    tp_arrive(norm_gather, tp_order[1:-1])
+    take([e for e in events if e[0] < 2])
 
     step_cols = share // depth
 
@@ -304,14 +321,13 @@
     def feed_one(i, _):
         @pl.when(i == 1)
         def _():
-            for k in range(tp - 1):
-                spread(k, peers[k], (tp_me + tp - 1 - k) % tp).wait_recv()
+            tp_arrive(norm_gather, tp_order[-1:])
 
         feed((side + i) % 2)
         return 0
 
     lax.fori_loop(0, 2, feed_one, 0)
-    take(len(events))
+    take(list(events))
 
     cols = wd_all.shape[2]
     ratio = share // cols
@@ -325,10 +341,10 @@
 
     used, pending = 0, []
 
-    def send(src, **target):
+    def send(src, dst, **target):
         nonlocal used
         copy = pltpu.make_async_remote_copy(
-            src_ref=src, dst_ref=rbuf.at[used], send_sem=red_send.at[used], recv_sem=red_recv.at[used],
+            src_ref=src, dst_ref=dst, send_sem=red_send.at[used], recv_sem=red_recv.at[used],
             device_id=target, device_id_type=MESH,
         )
         copy.start()
@@ -345,43 +361,53 @@
                     else:
                         channel[2 * m + where, :, s * cols : (s + 1) * cols] = value
                 if i == 0:
-                    send(sbuf.at[2 * m + where], tp=flip(tp_me, 1))
+                    send(sbuf.at[2 * m + where], rbuf.at[2 * m + where], tp=flip(tp_me, 1))
     for m in range(tp):
         pending[m].wait_recv()
         channel[m] = channel[m] + rbuf[m].astype(jnp.float32)
 
-    bit, sent = 2, 0
-    while bit < tp:
-        flag = (tp_me // bit) % 2
-        count = tp // (2 * bit)
+    strip = rows // 2
+    sent = 0
+    states = [{"bit": 2, "mate": False}, {"bit": 2, "mate": False}]
+    stages = len(tp_bits)
+    for stage in range(stages):
         batch = []
-        for m in range(count):
-            give = (tp_me % bit + bit * (1 - flag) + 2 * bit * m) // 2
-            keep = (tp_me % bit + bit * flag + 2 * bit * m) // 2
-            for i in range(2):
-                where = (1 - side) if i == 0 else side
-                tbuf[sent] = channel[2 * give + where].astype(jnp.bfloat16)
-                batch.append((used, 2 * keep + where))
-                send(tbuf.at[sent], tp=flip(tp_me, bit))
+        for lower in range(2):
+            state = states[lower]
+            at = pl.ds(lower * strip, strip)
+            bit = state["bit"]
+            moves = []
+            if stage == (0 if lower else stages - 1):
+                for q in range(tp // bit):
+                    d = (tp_me % bit + bit * q) // 2
+                    moves.append((2 * d + 1 - side, 2 * d + side))
+                state["mate"] = True
+                target = {"sp": mate}
+            else:
+                flag = (tp_me // bit) % 2
+                for m in range(tp // (2 * bit)):
+                    give = (tp_me % bit + bit * (1 - flag) + 2 * bit * m) // 2
+                    keep = (tp_me % bit + bit * flag + 2 * bit * m) // 2
+                    for where in [side] if state["mate"] else [1 - side, side]:
+                        moves.append((2 * give + where, 2 * keep + where))
+                state["bit"] = 2 * bit
+                target = {"tp": flip(tp_me, bit)}
+            for give, keep in moves:
+                tbuf[sent] = channel[give, at, :].astype(jnp.bfloat16)
+                batch.append((used, sent, keep, at))
+                send(tbuf.at[sent], ubuf.at[sent], **target)
                 sent += 1
-        for slot, keep in batch:
-            pending[slot].wait_recv()
-            channel[keep] = channel[keep] + rbuf[slot].astype(jnp.float32)
-        bit *= 2
-    tbuf[sent] = channel[2 * (tp_me // 2) + 1 - side].astype(jnp.bfloat16)
-    last = used
-    send(tbuf.at[sent], sp=mate)
-    pending[last].wait_recv()
-    final = channel[2 * (tp_me // 2) + side] + rbuf[last].astype(jnp.float32)
+        for index, slot, keep, at in batch:
+            pending[index].wait_recv()
+            channel[keep, at, :] = channel[keep, at, :] + ubuf[slot].astype(jnp.float32)
+    final = channel[2 * (tp_me // 2) + side]
     out[...] = (summed[tp_me] + 0.5 * final).astype(jnp.bfloat16)
 
     for copy in pending:
         copy.wait_send()
     swap(False).wait_send()
-    for k, peer in enumerate(peers):
-        out_copy(k, peer, tp_me).wait_send()
-        head_copy(k, peer, tp_me).wait_send()
-        spread(k, peer, tp_me).wait_send()
+    for gather in (out_gather, head_gather, norm_gather):
+        tp_drain(gather)
     for a in range(3):
         for mask in order[1:]:
             held, k = came[mask]
@@ -431,8 +457,9 @@
             pltpu.VMEM((2, rows, units // 2), bf16),
             pltpu.VMEM((tp, rows, share), f32),
             pltpu.VMEM((tp, rows, share), bf16),
-            pltpu.VMEM((2 * tp - 1, rows, share), bf16),
-            pltpu.VMEM((tp - 1, rows, share), bf16),
+            pltpu.VMEM((tp, rows, share), bf16),
+            pltpu.VMEM((2 * (tp - 1), rows // 2, share), bf16),
+            pltpu.VMEM((2 * (tp - 1), rows // 2, share), bf16),
             pltpu.VMEM((rows, 2 * hv), bf16),
             dma((7,)),
             dma((CHUNKS, 2, n - 1)),
@@ -443,10 +470,11 @@
             dma((tp - 1,)),
             dma((tp - 1,)),
             dma((tp - 1,)),
-            dma((tp,)),
-            dma((tp,)),
-            dma((2 * tp - 1,)),
-            dma((2 * tp - 1,)),
+            dma((2,)),
+            dma((tp - 1,)),
+            dma((tp - 1,)),
+            dma((3 * tp - 2,)),
+            dma((3 * tp - 2,)),
         ],
         compiler_params=pltpu.CompilerParams(
             collective_id=0, has_side_effects=True, vmem_limit_bytes=63 * 1024 * 1024

time: 220 us -> 197 us (0.90)
  Pallas kernels: 217 us -> 193 us
    pallas_call x1, Pallas kernels: 217 us -> 193 us  [local(): pl.pallas_call(functools.partial(kernel, n, tp), out_shape=jax.ShapeDtype...]
where the time goes in v3:
time: 197 us; the launch traced here: 196 us
  Pallas kernels  193 us (98%)
  local copies, waits for them, and re-layouts  3.06 us (2%)
    pallas_call x1, Pallas kernels, local(): pl.pallas_call(functools.partial(kernel, n, tp), out_shape=jax.ShapeDtype...  193 us

profile of v3, /device:TPU:0, one launch (start us, length us, event | category | flops | bytes accessed | tf_op | source)
XLA Modules:
  0.0 196.3 jit_solution(5485446516036533210)
XLA Ops:
  0.0 1.3 copy.16.lam
  1.3 193.2 %layer.1 = bf16[384,512]{1,0:T(8,128)(2,1)} custom-call(bf16[384,2048]{1,0:T(8,128)(2,1)} %residual.1, bf16[384,128]{1,0:T(8,128)(2,1)} %qa.1, bf16[384,128]{1,0:T(8,128)(2,1)} %ka.1, bf16[384,128]{1,0:T(8,128)(2,1)} %va.1, bf16[384,256]{1,0:T(8,128)(2,1)} %qb.1, bf16[384,256]{1,0:T(8,128)(2,1)} %kb.1, bf16[384,128]{1,0:T(8,128)(2,1)} %vb.1, ...), custom_call_target="tpu_custom_call" | custom-call | tf_op jit(solution)/shard_map/layer/pallas_call | solution.py:438
  194.5 1.8 copy.18
